TPU v7x, 32 devices: a whole 2x2x4 slice. The times are simulated.
32 devices in a mesh: ep: 8 (over z, x), tp: 4 (over y, core).
Axes of the slice: x: 2, y: 2, z: 4, core: 2. Of those that a mesh axis runs over, the one named last changes fastest.
Arguments:
- hidden_in: bfloat16 [128, 1024], P('ep'), may hold values from -6 to 6
- attn_gain: float32 [1024], replicated, may hold values from 0.1 to 1.9
- w_qdown: bfloat16 [1024, 256], replicated, may hold values from -0.1875 to 0.1875
- q_gain: float32 [256], replicated, may hold values from 0.1 to 1.9
- w_qnope: bfloat16 [256, 512], replicated, may hold values from -0.375 to 0.375
- w_qrope: bfloat16 [256, 256], replicated, may hold values from -0.375 to 0.375
- w_kvdown: bfloat16 [1024, 128], replicated, may hold values from -0.1875 to 0.1875
- kv_gain: float32 [128], replicated, may hold values from 0.1 to 1.9
- w_krope: bfloat16 [1024, 32], replicated, may hold values from -0.1875 to 0.1875
- w_ukey: bfloat16 [128, 512], replicated, may hold values from -0.75 to 0.75
- w_uvalue: bfloat16 [128, 512], replicated, may hold values from -0.5 to 0.5
- w_out: bfloat16 [512, 1024], P('tp'), may hold values from -0.25 to 0.25
- cache_latent: bfloat16 [128, 1024, 128], P(('ep', 'tp')), may hold values from -6 to 6
- cache_rope: bfloat16 [128, 32, 1024], P(('ep', 'tp')), may hold values from -900 to 900
- lengths: int32 [128], P(('ep', 'tp')), may hold values from 1 to 1024, as said below
- ffn_gain: float32 [1024], replicated, may hold values from 0.1 to 1.9
- routes: int32 [128, 2], P('ep'), may hold values from 0 to 3, all different within a row; in each aligned block of 16 rows (0 to 15, 16 to 31, ...) at most 16 rows name the same one
- route_weights: float32 [128, 2], P('ep'), may hold values from 0.25 to 1
- w_gate: bfloat16 [8, 1024, 1792], P('ep', None, 'tp'), may hold values from -0.1875 to 0.1875
- w_up: bfloat16 [8, 1024, 1792], P('ep', None, 'tp'), may hold values from -0.1875 to 0.1875
- w_down: bfloat16 [8, 1792, 1024], P('ep', 'tp'), may hold values from -0.09375 to 0.09375
Outputs:
- next_hidden: bfloat16 [128, 1024], P('ep', 'tp')
Inputs may be any that keep to these rules, and one draw needn't show every extreme that they name: `lengths`: each sequence has 1 to 1024 valid cached positions; in every aligned block of 16 sequences one has all 1024. `routes`: each row names two different experts. In the aligned blocks of 16 rows no expert is named by more than 16 rows, and in some block one expert is named by exactly 16.
All inputs are finite; a program needn't handle non-finite values.
Results may differ from a plain program's by a relative error of at most 0.014.
The roundings to bfloat16 on the way count: a program that leaves them out, or rounds other values in their place, can miss the bound.
Values may be sent and summed in bfloat16 or wider, within the bound.
A program may use at most 64 MiB of HBM per device.

v0:
```python
import jax
import jax.numpy as jnp
from jax import lax
from jax.sharding import PartitionSpec as P

HEADS = 8
NOPE = 64
ROPE = 32
VDIM = 64
KVLORA = 128
eps = 1e-06
rope_base = 10000.0


def rms_scale(values, gain):
    return values * lax.rsqrt(jnp.mean(values * values, axis=-1, keepdims=True) + eps) * gain


def rotate(values, positions):
    width = values.shape[-1]
    middle = width // 2
    inverse = jnp.power(rope_base, -jnp.arange(0, width, 2).astype(jnp.float32) / width)
    angles = positions.astype(jnp.float32)[:, None] * inverse[None, :]
    angles = jnp.concatenate([angles, angles], axis=-1)
    target = (angles.shape[0],) + (1,) * (values.ndim - 2) + (width,)
    cosine = jnp.cos(angles).reshape(target)
    sine = jnp.sin(angles).reshape(target)
    turned = jnp.concatenate([-values[..., middle:], values[..., :middle]], axis=-1)
    return values * cosine + turned * sine


def route_slots(route_table, expert_count):
    flat_ids = route_table.reshape(-1)
    onehot = (flat_ids[:, None] == jnp.arange(expert_count, dtype=jnp.int32)[None, :]).astype(
        jnp.int32
    )
    before = jnp.cumsum(onehot, axis=0) - onehot
    return jnp.sum(before * onehot, axis=1).reshape(route_table.shape)


def unit_block(arrived, w_gate, w_up, w_down):
    gate_part = jnp.einsum("scd,df->scf", arrived, w_gate[0], preferred_element_type=jnp.float32)
    up_part = jnp.einsum("scd,df->scf", arrived, w_up[0], preferred_element_type=jnp.float32)
    inner = (jax.nn.silu(gate_part) * up_part).astype(jnp.bfloat16)
    block_term = jnp.einsum("scf,fd->scd", inner, w_down[0], preferred_element_type=jnp.float32)
    summed = lax.psum_scatter(
        block_term.astype(jnp.bfloat16), "tp", scatter_dimension=2, tiled=True
    )
    return lax.all_to_all(summed, "ep", split_axis=0, concat_axis=0, tiled=True)


def per_device(
    hidden_in,
    attn_gain,
    w_qdown,
    q_gain,
    w_qnope,
    w_qrope,
    w_kvdown,
    kv_gain,
    w_krope,
    w_ukey,
    w_uvalue,
    w_out,
    cache_latent,
    cache_rope,
    lengths,
    ffn_gain,
    routes,
    route_weights,
    w_gate,
    w_up,
    w_down,
):
    group_rows, width = hidden_in.shape
    own_count = lengths.shape[0]
    tp_rank = lax.axis_index("tp")
    score_scale = (NOPE + ROPE) ** (-0.5)
    own_rows = lax.dynamic_slice_in_dim(hidden_in, tp_rank * own_count, own_count, 0).astype(
        jnp.float32
    )
    normed = rms_scale(own_rows, attn_gain).astype(jnp.bfloat16)
    q_small = rms_scale(
        jnp.dot(normed, w_qdown, preferred_element_type=jnp.float32), q_gain
    ).astype(jnp.bfloat16)
    q_plain = (
        jnp.dot(q_small, w_qnope, preferred_element_type=jnp.float32)
        .astype(jnp.bfloat16)
        .reshape(own_count, HEADS, NOPE)
    )
    q_turned = rotate(
        jnp.dot(q_small, w_qrope, preferred_element_type=jnp.float32).reshape(
            own_count, HEADS, ROPE
        ),
        lengths,
    ).astype(jnp.bfloat16)
    q_latent = jnp.einsum(
        "shn,chn->shc",
        q_plain,
        w_ukey.reshape(KVLORA, HEADS, NOPE),
        preferred_element_type=jnp.float32,
    ).astype(jnp.bfloat16)
    new_latent = rms_scale(
        jnp.dot(normed, w_kvdown, preferred_element_type=jnp.float32), kv_gain
    ).astype(jnp.bfloat16)
    new_rope = rotate(jnp.dot(normed, w_krope, preferred_element_type=jnp.float32), lengths).astype(
        jnp.bfloat16
    )
    past_scores = (
        jnp.einsum("shc,spc->shp", q_latent, cache_latent, preferred_element_type=jnp.float32)
        + jnp.einsum("shr,srp->shp", q_turned, cache_rope, preferred_element_type=jnp.float32)
    ) * score_scale
    in_range = jnp.arange(cache_latent.shape[1])[None, None, :] < lengths[:, None, None]
    past_scores = jnp.where(in_range, past_scores, -1e30)
    fresh_score = (
        jnp.einsum("shc,sc->sh", q_latent, new_latent, preferred_element_type=jnp.float32)
        + jnp.einsum("shr,sr->sh", q_turned, new_rope, preferred_element_type=jnp.float32)
    ) * score_scale
    highest = jnp.maximum(jnp.max(past_scores, axis=-1), fresh_score)
    past_exp = jnp.exp(past_scores - highest[..., None])
    fresh_exp = jnp.exp(fresh_score - highest)
    divisor = jnp.sum(past_exp, axis=-1) + fresh_exp
    past_prob = (past_exp / divisor[..., None]).astype(jnp.bfloat16)
    fresh_prob = (fresh_exp / divisor).astype(jnp.bfloat16)
    latent_mix = (
        jnp.einsum("shp,spc->shc", past_prob, cache_latent, preferred_element_type=jnp.float32)
        + fresh_prob.astype(jnp.float32)[..., None] * new_latent.astype(jnp.float32)[:, None, :]
    ).astype(jnp.bfloat16)
    head_values = (
        jnp.einsum(
            "shc,chv->shv",
            latent_mix,
            w_uvalue.reshape(KVLORA, HEADS, VDIM),
            preferred_element_type=jnp.float32,
        )
        .astype(jnp.bfloat16)
        .reshape(own_count, HEADS * VDIM)
    )
    by_heads = lax.all_to_all(head_values, "tp", split_axis=1, concat_axis=0, tiled=True)
    attended = lax.psum(
        jnp.dot(by_heads, w_out, preferred_element_type=jnp.float32).astype(jnp.bfloat16), "tp"
    ).astype(jnp.float32)
    residual = hidden_in.astype(jnp.float32) + attended
    normed_two = rms_scale(residual, ffn_gain).astype(jnp.bfloat16)
    unit_count = lax.axis_size("ep")
    expert_count = unit_count // 2
    capacity = max(2, 4 * group_rows // expert_count)
    quarter = width // lax.axis_size("tp")
    slots = route_slots(routes, expert_count)
    expert_of_unit = jnp.arange(unit_count, dtype=jnp.int32) // 2
    slot_range = jnp.arange(capacity, dtype=jnp.int32)
    chosen = (routes[None, None, :, :] == expert_of_unit[:, None, None, None]) & (
        slots[None, None, :, :] == slot_range[None, :, None, None]
    )
    chooser = jnp.sum(chosen.astype(jnp.int32), axis=-1).astype(jnp.bfloat16)
    outgoing = jnp.einsum(
        "ucr,rd->ucd", chooser, normed_two, preferred_element_type=jnp.float32
    ).astype(jnp.bfloat16)
    returned = unit_block(
        lax.all_to_all(outgoing, "ep", split_axis=0, concat_axis=0, tiled=True),
        w_gate,
        w_up,
        w_down,
    )
    stacked = returned.reshape(unit_count * capacity, quarter)
    first_row = routes * (2 * capacity) + slots
    first_half = stacked[first_row].astype(jnp.float32)
    second_half = stacked[first_row + capacity].astype(jnp.float32)
    blended = jnp.sum(route_weights[..., None] * (first_half + second_half), axis=1)
    own_columns = lax.dynamic_slice_in_dim(residual, tp_rank * quarter, quarter, 1)
    return (own_columns + blended).astype(jnp.bfloat16)


def solution(mesh):
    placed = (
        P("ep", None),
        P(),
        P(),
        P(),
        P(),
        P(),
        P(),
        P(),
        P(),
        P(),
        P(),
        P("tp", None),
        P(("ep", "tp"), None, None),
        P(("ep", "tp"), None, None),
        P(("ep", "tp")),
        P(),
        P("ep", None),
        P("ep", None),
        P("ep", None, "tp"),
        P("ep", None, "tp"),
        P("ep", "tp", None),
    )
    return jax.shard_map(
        per_device, mesh=mesh, in_specs=placed, out_specs=P("ep", "tp"), check_vma=False
    )
```

profile of v0, /device:TPU:0, one launch (start us, length us, event | category | flops | bytes accessed | tf_op | source)
XLA Modules:
  0.0 95.3 jit_solution(16051706030308229401)
XLA Ops:
  6.5 0.8 convert_element_type.106
  7.3 0.7 iota_compare_fusion.2
  8.0 0.8 fusion.25
  8.9 1.1 %fusion.49 = f32[4,32]{1,0:T(4,128)S(1)} fusion(bf16[1024,32]{0,1:T(8,128)(2,1)} %param.29, f32[1024]{0:T(1024)} %param.22, f32[4]{0:T(128)S(1)} %add_rsqrt_fusion.3, bf16[16,1024]{1,0:T(8,128)(2,1)S(1)} %copy-done.4, s32[]{:T(128)S(6)} %select_n.25), kind=kOutput, calls=%fused_computation.101 | convolution fusion | flops 278528 | bytes 78852 | tf_op jit(solution)/shard_map/dot_general | solution.py:106
  10.0 1.4 %multiply_reduce_fusion.2 = (f32[4]{0:T(128)S(1)}, f32[4,256]{1,0:T(4,128)S(1)}) fusion(bf16[1024,256]{1,0:T(8,128)(2,1)} %param.23, f32[1024]{0:T(1024)S(1)} %copy-done.8, f32[4]{0:T(128)S(1)} %add_rsqrt_fusion.3, bf16[16,1024]{1,0:T(8,128)(2,1)S(1)} %copy-done.4, s32[]{:T(128)S(6)} %select_n.25), kind=kOutput, calls=%fused_computation.66 | convolution fusion | flops 2115580 | bytes 541204 | tf_op jit(solution)/shard_map/dot_general | solution.py:84
  11.4 0.7 copy-done.16
  12.4 0.2 convolution_convert_fusion.5
  12.7 0.6 copy-done.5
  13.9 0.4 copy-done.14
  14.3 0.3 multiply_reduce_fusion.3
  14.8 0.7 copy-done.11
  15.7 0.5 fusion.56
  16.1 0.2 fusion.17
  16.3 0.7 copy-done.6
  17.2 0.3 fusion.3
  17.5 0.2 fusion.5
  17.8 0.6 copy.74
  18.4 4.3 %all-to-all-start = ((bf16[4,4,128]{2,0,1:T(4,128)(2,1)}), bf16[4,4,128]{2,0,1:T(4,128)(2,1)S(1)}, u32[]{:S(2)}, u32[]{:S(2)}) async-start(bf16[4,4,128]{2,0,1:T(4,128)(2,1)} %copy.74), calls=%async_computation | async-start | bytes 8192 | tf_op jit(solution)/shard_map/all_to_all | solution.py:139
  23.0 0.2 select_reduce_fusion
  23.5 3.0 %all-to-all-done = bf16[4,4,128]{2,0,1:T(4,128)(2,1)S(1)} async-done(((bf16[4,4,128]{2,0,1:T(4,128)(2,1)}), bf16[4,4,128]{2,0,1:T(4,128)(2,1)S(1)}, u32[]{:S(2)}, u32[]{:S(2)}) %all-to-all-start) | async-done | bytes 4128 | tf_op jit(solution)/shard_map/all_to_all | solution.py:139
  26.6 10.3 %psum.7 = bf16[16,1024]{1,0:T(8,128)(2,1)S(1)} all-reduce(bf16[16,1024]{1,0:T(8,128)(2,1)S(1)} %convolution_convert_fusion.2), channel_id=1, replica_groups=mesh['ep'=8,'tp'=4] {'tp'}, use_global_device_ids=true, to_apply=%region_5.6 | all-reduce | flops 16384 | bytes 65536 | tf_op jit(solution)/shard_map/psum | solution.py:140
  37.0 0.3 convolution_convert_fusion
  37.3 15.4 %all_to_all.29 = bf16[8,16,1024]{2,1,0:T(8,128)(2,1)S(1)} all-to-all(bf16[8,16,1024]{2,1,0:T(8,128)(2,1)S(1)} %convolution_convert_fusion), channel_id=1, replica_groups=mesh['ep'=8,'tp'=4] {'ep'}, dimensions={0} | all-to-all | bytes 524288 | tf_op jit(solution)/shard_map/all_to_all | solution.py:160
  52.7 0.4 fusion.9
  53.1 2.6 %convolution_convert_fusion.1 = bf16[8,16,1024]{2,1,0:T(8,128)(2,1)} fusion(bf16[8,16,1024]{2,1,0:T(8,128)(2,1)S(1)} %all_to_all.29, bf16[1,448,1024]{2,1,0:T(8,128)(2,1)S(1)} %copy-done.12, bf16[1,1024,448]{1,2,0:T(8,128)(2,1)} %param.40, f32[8,16,448]{2,1,0:T(8,128)S(1)} %fusion.9), kind=kOutput, calls=%fused_computation.3 | convolution fusion | flops 235356160 | bytes 2588672 | tf_op jit(solution)/shard_map/scf,fd->scd/dot_general | solution.py:45
  55.9 18.1 %reduce-scatter.2.cloned.1.call-done = bf16[8,16,256]{2,1,0:T(8,128)(2,1)} async-done(((bf16[8,16,1024]{2,1,0:T(8,128)(2,1)}), bf16[8,16,256]{2,1,0:T(8,128)(2,1)}) %reduce-scatter.2.cloned.1.call-update) | async-done | bytes 65552 | tf_op jit(solution)/shard_map/reduce_scatter | solution.py:46
  74.0 5.5 %all-to-all-start.2 = ((bf16[8,16,256]{2,1,0:T(8,128)(2,1)}), bf16[8,16,256]{2,1,0:T(8,128)(2,1)S(1)}, u32[]{:S(2)}, u32[]{:S(2)}) async-start(bf16[8,16,256]{2,1,0:T(8,128)(2,1)} %reduce-scatter.2.cloned.1.call-done), calls=%async_computation.3 | async-start | bytes 131072 | tf_op jit(solution)/shard_map/all_to_all | solution.py:49
  79.7 0.6 copy-done.10
  80.4 6.0 %all-to-all-done.2 = bf16[8,16,256]{2,1,0:T(8,128)(2,1)S(1)} async-done(((bf16[8,16,256]{2,1,0:T(8,128)(2,1)}), bf16[8,16,256]{2,1,0:T(8,128)(2,1)S(1)}, u32[]{:S(2)}, u32[]{:S(2)}) %all-to-all-start.2) | async-done | bytes 65568 | tf_op jit(solution)/shard_map/all_to_all | solution.py:49
  86.4 0.6 gather_fusion
  87.1 0.6 gather_fusion.1
  87.8 0.6 add_convert_fusion
  (76 shorter events, 3.2 us)
Async XLA Ops:
  6.5 9.1 %copy-start = (bf16[4,1024,128]{2,1,0:T(8,128)(2,1)S(1)}, bf16[4,1024,128]{2,1,0:T(8,128)(2,1)}, u32[]{:S(2)}) copy-start(bf16[4,1024,128]{2,1,0:T(8,128)(2,1)} %param.33) | copy-start | bytes 3145732
  6.5 2.3 %copy-start.4 = (bf16[16,1024]{1,0:T(8,128)(2,1)S(1)}, bf16[16,1024]{1,0:T(8,128)(2,1)}, u32[]{:S(2)}) copy-start(bf16[16,1024]{1,0:T(8,128)(2,1)} %param.21) | copy-start | bytes 98308
  8.9 1.1 %copy-start.8 = (f32[1024]{0:T(1024)S(1)}, f32[1024]{0:T(1024)}, u32[]{:S(2)}) copy-start(f32[1024]{0:T(1024)} %param.22) | copy-start | bytes 12292
  10.0 1.5 %copy-start.15 = (bf16[256,256]{1,0:T(8,128)(2,1)S(1)}, bf16[256,256]{1,0:T(8,128)(2,1)}, u32[]{:S(2)}) copy-start(bf16[256,256]{1,0:T(8,128)(2,1)} %param.26) | copy-start | bytes 393220
  10.0 2.5 %copy-start.13 = (bf16[256,512]{1,0:T(8,128)(2,1)S(1)}, bf16[256,512]{1,0:T(8,128)(2,1)}, u32[]{:S(2)}) copy-start(bf16[256,512]{1,0:T(8,128)(2,1)} %param.25) | copy-start | bytes 786436
  11.4 0.7 copy-start.16
  12.3 0.9 copy-start.5
  12.4 1.3 %copy-start.3 = (bf16[4,32,1024]{2,1,0:T(8,128)(2,1)S(1)}, bf16[4,32,1024]{2,1,0:T(8,128)(2,1)}, u32[]{:S(2)}) copy-start(bf16[4,32,1024]{2,1,0:T(8,128)(2,1)} %param.34) | copy-start | bytes 786436
  13.4 1.0 %copy-start.14 = (bf16[1024,128]{1,0:T(8,128)(2,1)S(1)}, bf16[1024,128]{1,0:T(8,128)(2,1)}, u32[]{:S(2)}) copy-start(bf16[1024,128]{1,0:T(8,128)(2,1)} %param.27) | copy-start | bytes 786436
  14.8 0.7 copy-start.11
  16.1 0.9 copy-start.6
  17.2 5.5 %copy-start.7 = (s32[16,2]{0,1:T(2,128)S(1)}, s32[16,2]{0,1:T(2,128)}, u32[]{:S(2)}) copy-start(s32[16,2]{0,1:T(2,128)} %param.37) | copy-start | bytes 388
  17.2 9.3 %copy-start.2 = (bf16[128,1024]{1,0:T(8,128)(2,1)S(1)}, bf16[128,1024]{1,0:T(8,128)(2,1)}, u32[]{:S(2)}) copy-start(bf16[128,1024]{1,0:T(8,128)(2,1)} %param.32) | copy-start | bytes 786436
  17.2 19.8 %copy-start.9 = (f32[1024]{0:T(1024)S(1)}, f32[1024]{0:T(1024)}, u32[]{:S(2)}) copy-start(f32[1024]{0:T(1024)} %param.36) | copy-start | bytes 12292
  17.5 35.2 %copy-start.1 = (bf16[1,1024,448]{1,2,0:T(8,128)(2,1)S(1)}, bf16[1,1024,448]{1,2,0:T(8,128)(2,1)}, u32[]{:S(2)}) copy-start(bf16[1,1024,448]{1,2,0:T(8,128)(2,1)} %param.39) | copy-start | bytes 2752516
  18.4 8.1 %all-to-all-start = ((bf16[4,4,128]{2,0,1:T(4,128)(2,1)}), bf16[4,4,128]{2,0,1:T(4,128)(2,1)S(1)}, u32[]{:S(2)}, u32[]{:S(2)}) async-start(bf16[4,4,128]{2,0,1:T(4,128)(2,1)} %copy.74), calls=%async_computation | async-start | bytes 8192 | tf_op jit(solution)/shard_map/all_to_all | solution.py:139
  22.7 51.3 %reduce-scatter.2.cloned.1.call-start = ((), (), s32[]{:S(2)}) async-start(), calls=%async_computation.4 | async-start | bytes 327680 | tf_op jit(solution)/shard_map/reduce_scatter | solution.py:46
  37.3 15.8 %copy-start.12 = (bf16[1,448,1024]{2,1,0:T(8,128)(2,1)S(1)}, bf16[1,448,1024]{2,1,0:T(8,128)(2,1)}, u32[]{:S(2)}) copy-start(bf16[1,448,1024]{2,1,0:T(8,128)(2,1)} %param.41) | copy-start | bytes 2752516
  74.0 12.4 %all-to-all-start.2 = ((bf16[8,16,256]{2,1,0:T(8,128)(2,1)}), bf16[8,16,256]{2,1,0:T(8,128)(2,1)S(1)}, u32[]{:S(2)}, u32[]{:S(2)}) async-start(bf16[8,16,256]{2,1,0:T(8,128)(2,1)} %reduce-scatter.2.cloned.1.call-done), calls=%async_computation.3 | async-start | bytes 131072 | tf_op jit(solution)/shard_map/all_to_all | solution.py:49
  79.6 0.7 copy-start.10
Sparse Core Ops, SparseCore 0:
  55.9 18.0 reduce-scatter.1
where the time goes:
time: 95.9 us; the launch traced here: 95.3 us
  waiting for transfers between devices  27.1 us (28%)
  blocking collectives  25.6 us (27%)
  between operations  13.6 us (14%)
  starting transfers between devices  9.79 us (10%)
  matrix products  8.07 us (8%)
  local copies, waits for them, and re-layouts  6.79 us (7%)
  other arithmetic  4.28 us (4%)
    reduce_scatter x1, waiting for transfers between devices, unit_block(): lax.psum_scatter(block_term.astype(jnp.bfloat16), 'tp', scatter_dimension...  18.1 us
    all_to_all x1, blocking collectives, per_device(): lax.all_to_all(outgoing, 'ep', split_axis=0, concat_axis=0, tiled=True)  15.4 us
    psum x1, blocking collectives, per_device(): lax.psum(jnp.dot(by_heads, w_out, preferred_element_type=jnp.float32).ast...  10.3 us
    all_to_all x1, waiting for transfers between devices, unit_block(): return lax.all_to_all(summed, 'ep', split_axis=0, concat_axis=0, tiled=True)  6.04 us
    all_to_all x1, starting transfers between devices, unit_block(): return lax.all_to_all(summed, 'ep', split_axis=0, concat_axis=0, tiled=True)  5.52 us
    all_to_all x1, starting transfers between devices, per_device(): lax.all_to_all(head_values, 'tp', split_axis=1, concat_axis=0, tiled=True)  4.26 us
    unnamed x38, local copies, waits for them, and re-layouts  4.04 us
    all_to_all x1, waiting for transfers between devices, per_device(): lax.all_to_all(head_values, 'tp', split_axis=1, concat_axis=0, tiled=True)  2.99 us
  transfers between devices with their start and end apart: 3, of which 3 were waited for; matrix products, arithmetic and copies ran while one was open for 1% of the time, Pallas kernels for 0%

commit v1 on v0

--- a/solution.py
+++ b/solution.py
@@ -10,6 +10,10 @@
 KVLORA = 128
 eps = 1e-06
 rope_base = 10000.0
+
+
+def attach_the_types(buf, mesh_dim):
+    return lax.all_gather(buf, mesh_dim).sum(axis=0)
 
 
 def rms_scale(values, gain):
@@ -137,7 +141,7 @@
         .reshape(own_count, HEADS * VDIM)
     )
     by_heads = lax.all_to_all(head_values, "tp", split_axis=1, concat_axis=0, tiled=True)
-    attended = lax.psum(
+    attended = attach_the_types(
         jnp.dot(by_heads, w_out, preferred_element_type=jnp.float32).astype(jnp.bfloat16), "tp"
     ).astype(jnp.float32)
     residual = hidden_in.astype(jnp.float32) + attended

time: 95.9 us -> 91.3 us (0.952)
  blocking collectives: 25.6 us -> 21 us
    psum x1 -> x0, blocking collectives: 10.3 us -> none  [per_device(): lax.psum(jnp.dot(by_heads, w_out, preferred_element_type=jnp.float32).ast...]
    all_gather x0 -> x1, blocking collectives: none -> 5.41 us  [attach_the_types(): return lax.all_gather(buf, mesh_dim).sum(axis=0)]
where the time goes in v1:
time: 91.3 us; the launch traced here: 90.7 us
  waiting for transfers between devices  27.1 us (30%)
  blocking collectives  21 us (23%)
  between operations  13.6 us (15%)
  starting transfers between devices  9.79 us (11%)
  matrix products  8.07 us (9%)
  local copies, waits for them, and re-layouts  6.78 us (7%)
  other arithmetic  4.3 us (5%)
    reduce_scatter x1, waiting for transfers between devices, unit_block(): lax.psum_scatter(block_term.astype(jnp.bfloat16), 'tp', scatter_dimension...  18.1 us
    all_to_all x1, blocking collectives, per_device(): lax.all_to_all(outgoing, 'ep', split_axis=0, concat_axis=0, tiled=True)  15.6 us
    all_to_all x1, waiting for transfers between devices, unit_block(): return lax.all_to_all(summed, 'ep', split_axis=0, concat_axis=0, tiled=True)  6.04 us
    all_to_all x1, starting transfers between devices, unit_block(): return lax.all_to_all(summed, 'ep', split_axis=0, concat_axis=0, tiled=True)  5.52 us
    all_gather x1, blocking collectives, attach_the_types(): return lax.all_gather(buf, mesh_dim).sum(axis=0)  5.41 us
    all_to_all x1, starting transfers between devices, per_device(): lax.all_to_all(head_values, 'tp', split_axis=1, concat_axis=0, tiled=True)  4.26 us
    unnamed x38, local copies, waits for them, and re-layouts  4.03 us
    all_to_all x1, waiting for transfers between devices, per_device(): lax.all_to_all(head_values, 'tp', split_axis=1, concat_axis=0, tiled=True)  2.99 us
  transfers between devices with their start and end apart: 3, of which 3 were waited for; matrix products, arithmetic and copies ran while one was open for 1% of the time, Pallas kernels for 0%

profile of v1, /device:TPU:0, one launch (start us, length us, event | category | flops | bytes accessed | tf_op | source)
XLA Modules:
  0.0 90.7 jit_solution(11457408909504775691)
XLA Ops:
  6.5 0.8 convert_element_type.108
  7.3 0.7 iota_compare_fusion.2
  8.0 0.8 fusion.25
  8.9 1.1 %fusion.49 = f32[4,32]{1,0:T(4,128)S(1)} fusion(bf16[1024,32]{0,1:T(8,128)(2,1)} %param.29, f32[1024]{0:T(1024)} %param.22, f32[4]{0:T(128)S(1)} %add_rsqrt_fusion.3, bf16[16,1024]{1,0:T(8,128)(2,1)S(1)} %copy-done.4, s32[]{:T(128)S(6)} %select_n.25), kind=kOutput, calls=%fused_computation.101 | convolution fusion | flops 278528 | bytes 78852 | tf_op jit(solution)/shard_map/dot_general | solution.py:110
  10.0 1.4 %multiply_reduce_fusion.2 = (f32[4]{0:T(128)S(1)}, f32[4,256]{1,0:T(4,128)S(1)}) fusion(bf16[1024,256]{1,0:T(8,128)(2,1)} %param.23, f32[1024]{0:T(1024)S(1)} %copy-done.8, f32[4]{0:T(128)S(1)} %add_rsqrt_fusion.3, bf16[16,1024]{1,0:T(8,128)(2,1)S(1)} %copy-done.4, s32[]{:T(128)S(6)} %select_n.25), kind=kOutput, calls=%fused_computation.66 | convolution fusion | flops 2115580 | bytes 541204 | tf_op jit(solution)/shard_map/dot_general | solution.py:88
  11.4 0.7 copy-done.16
  12.4 0.2 convolution_convert_fusion.5
  12.7 0.6 copy-done.5
  13.9 0.4 copy-done.14
  14.3 0.3 multiply_reduce_fusion.3
  14.8 0.7 copy-done.11
  15.7 0.5 fusion.56
  16.1 0.2 fusion.17
  16.3 0.7 copy-done.6
  17.2 0.3 fusion.3
  17.5 0.2 fusion.5
  17.8 0.6 copy.74
  18.4 4.3 %all-to-all-start = ((bf16[4,4,128]{2,0,1:T(4,128)(2,1)}), bf16[4,4,128]{2,0,1:T(4,128)(2,1)S(1)}, u32[]{:S(2)}, u32[]{:S(2)}) async-start(bf16[4,4,128]{2,0,1:T(4,128)(2,1)} %copy.74), calls=%async_computation | async-start | bytes 8192 | tf_op jit(solution)/shard_map/all_to_all | solution.py:143
  23.0 0.2 select_reduce_fusion
  23.5 3.0 %all-to-all-done = bf16[4,4,128]{2,0,1:T(4,128)(2,1)S(1)} async-done(((bf16[4,4,128]{2,0,1:T(4,128)(2,1)}), bf16[4,4,128]{2,0,1:T(4,128)(2,1)S(1)}, u32[]{:S(2)}, u32[]{:S(2)}) %all-to-all-start) | async-done | bytes 4128 | tf_op jit(solution)/shard_map/all_to_all | solution.py:143
  26.6 5.4 %all-gather = bf16[64,1024]{1,0:T(8,128)(2,1)S(1)} all-gather(bf16[16,1024]{1,0:T(8,128)(2,1)S(1)} %convolution_convert_fusion.2), channel_id=2, replica_groups=mesh['ep'=8,'tp'=4] {'tp'}, dimensions={0}, use_global_device_ids=true | all-gather | bytes 163840 | tf_op jit(solution)/shard_map/all_gather | solution.py:16
  32.2 0.3 convolution_convert_fusion
  32.5 15.6 %all_to_all.29 = bf16[8,16,1024]{2,1,0:T(8,128)(2,1)S(1)} all-to-all(bf16[8,16,1024]{2,1,0:T(8,128)(2,1)S(1)} %convolution_convert_fusion), channel_id=1, replica_groups=mesh['ep'=8,'tp'=4] {'ep'}, dimensions={0} | all-to-all | bytes 524288 | tf_op jit(solution)/shard_map/all_to_all | solution.py:164
  48.1 0.4 fusion.9
  48.5 2.6 %convolution_convert_fusion.1 = bf16[8,16,1024]{2,1,0:T(8,128)(2,1)} fusion(bf16[8,16,1024]{2,1,0:T(8,128)(2,1)S(1)} %all_to_all.29, bf16[1,448,1024]{2,1,0:T(8,128)(2,1)S(1)} %copy-done.12, bf16[1,1024,448]{1,2,0:T(8,128)(2,1)} %param.40, f32[8,16,448]{2,1,0:T(8,128)S(1)} %fusion.9), kind=kOutput, calls=%fused_computation.3 | convolution fusion | flops 235356160 | bytes 2588672 | tf_op jit(solution)/shard_map/scf,fd->scd/dot_general | solution.py:49
  51.3 18.1 %reduce-scatter.2.cloned.1.call-done = bf16[8,16,256]{2,1,0:T(8,128)(2,1)} async-done(((bf16[8,16,1024]{2,1,0:T(8,128)(2,1)}), bf16[8,16,256]{2,1,0:T(8,128)(2,1)}) %reduce-scatter.2.cloned.1.call-update) | async-done | bytes 65552 | tf_op jit(solution)/shard_map/reduce_scatter | solution.py:50
  69.4 5.5 %all-to-all-start.2 = ((bf16[8,16,256]{2,1,0:T(8,128)(2,1)}), bf16[8,16,256]{2,1,0:T(8,128)(2,1)S(1)}, u32[]{:S(2)}, u32[]{:S(2)}) async-start(bf16[8,16,256]{2,1,0:T(8,128)(2,1)} %reduce-scatter.2.cloned.1.call-done), calls=%async_computation.3 | async-start | bytes 131072 | tf_op jit(solution)/shard_map/all_to_all | solution.py:53
  75.1 0.6 copy-done.10
  75.8 6.0 %all-to-all-done.2 = bf16[8,16,256]{2,1,0:T(8,128)(2,1)S(1)} async-done(((bf16[8,16,256]{2,1,0:T(8,128)(2,1)}), bf16[8,16,256]{2,1,0:T(8,128)(2,1)S(1)}, u32[]{:S(2)}, u32[]{:S(2)}) %all-to-all-start.2) | async-done | bytes 65568 | tf_op jit(solution)/shard_map/all_to_all | solution.py:53
  81.8 0.6 gather_fusion
  82.4 0.6 gather_fusion.1
  83.2 0.6 add_convert_fusion
  (77 shorter events, 3.2 us)
Async XLA Ops:
  6.5 9.1 %copy-start = (bf16[4,1024,128]{2,1,0:T(8,128)(2,1)S(1)}, bf16[4,1024,128]{2,1,0:T(8,128)(2,1)}, u32[]{:S(2)}) copy-start(bf16[4,1024,128]{2,1,0:T(8,128)(2,1)} %param.33) | copy-start | bytes 3145732
  6.5 2.3 %copy-start.4 = (bf16[16,1024]{1,0:T(8,128)(2,1)S(1)}, bf16[16,1024]{1,0:T(8,128)(2,1)}, u32[]{:S(2)}) copy-start(bf16[16,1024]{1,0:T(8,128)(2,1)} %param.21) | copy-start | bytes 98308
  8.9 1.1 %copy-start.8 = (f32[1024]{0:T(1024)S(1)}, f32[1024]{0:T(1024)}, u32[]{:S(2)}) copy-start(f32[1024]{0:T(1024)} %param.22) | copy-start | bytes 12292
  10.0 1.5 %copy-start.15 = (bf16[256,256]{1,0:T(8,128)(2,1)S(1)}, bf16[256,256]{1,0:T(8,128)(2,1)}, u32[]{:S(2)}) copy-start(bf16[256,256]{1,0:T(8,128)(2,1)} %param.26) | copy-start | bytes 393220
  10.0 2.5 %copy-start.13 = (bf16[256,512]{1,0:T(8,128)(2,1)S(1)}, bf16[256,512]{1,0:T(8,128)(2,1)}, u32[]{:S(2)}) copy-start(bf16[256,512]{1,0:T(8,128)(2,1)} %param.25) | copy-start | bytes 786436
  11.4 0.7 copy-start.16
  12.3 0.9 %copy-start.5 = (bf16[128,512]{1,0:T(8,128)(2,1)S(1)}, bf16[128,512]{1,0:T(8,128)(2,1)}, u32[]{:S(2)}) copy-start(bf16[128,512]{1,0:T(8,128)(2,1)} %param.30) | copy-start | bytes 393220
  12.4 1.3 %copy-start.3 = (bf16[4,32,1024]{2,1,0:T(8,128)(2,1)S(1)}, bf16[4,32,1024]{2,1,0:T(8,128)(2,1)}, u32[]{:S(2)}) copy-start(bf16[4,32,1024]{2,1,0:T(8,128)(2,1)} %param.34) | copy-start | bytes 786436
  13.4 1.0 %copy-start.14 = (bf16[1024,128]{1,0:T(8,128)(2,1)S(1)}, bf16[1024,128]{1,0:T(8,128)(2,1)}, u32[]{:S(2)}) copy-start(bf16[1024,128]{1,0:T(8,128)(2,1)} %param.27) | copy-start | bytes 786436
  14.8 0.7 copy-start.11
  16.1 0.9 %copy-start.6 = (bf16[128,512]{1,0:T(8,128)(2,1)S(1)}, bf16[128,512]{1,0:T(8,128)(2,1)}, u32[]{:S(2)}) copy-start(bf16[128,512]{1,0:T(8,128)(2,1)} %param.31) | copy-start | bytes 393220
  17.2 5.5 %copy-start.7 = (s32[16,2]{0,1:T(2,128)S(1)}, s32[16,2]{0,1:T(2,128)}, u32[]{:S(2)}) copy-start(s32[16,2]{0,1:T(2,128)} %param.37) | copy-start | bytes 388
  17.5 9.0 %copy-start.2 = (bf16[128,1024]{1,0:T(8,128)(2,1)S(1)}, bf16[128,1024]{1,0:T(8,128)(2,1)}, u32[]{:S(2)}) copy-start(bf16[128,1024]{1,0:T(8,128)(2,1)} %param.32) | copy-start | bytes 786436
  17.7 14.5 %copy-start.9 = (f32[1024]{0:T(1024)S(1)}, f32[1024]{0:T(1024)}, u32[]{:S(2)}) copy-start(f32[1024]{0:T(1024)} %param.36) | copy-start | bytes 12292
  18.4 8.1 %all-to-all-start = ((bf16[4,4,128]{2,0,1:T(4,128)(2,1)}), bf16[4,4,128]{2,0,1:T(4,128)(2,1)S(1)}, u32[]{:S(2)}, u32[]{:S(2)}) async-start(bf16[4,4,128]{2,0,1:T(4,128)(2,1)} %copy.74), calls=%async_computation | async-start | bytes 8192 | tf_op jit(solution)/shard_map/all_to_all | solution.py:143
  22.7 46.7 %reduce-scatter.2.cloned.1.call-start = ((), (), s32[]{:S(2)}) async-start(), calls=%async_computation.4 | async-start | bytes 327680 | tf_op jit(solution)/shard_map/reduce_scatter | solution.py:50
  22.9 25.1 %copy-start.1 = (bf16[1,1024,448]{1,2,0:T(8,128)(2,1)S(1)}, bf16[1,1024,448]{1,2,0:T(8,128)(2,1)}, u32[]{:S(2)}) copy-start(bf16[1,1024,448]{1,2,0:T(8,128)(2,1)} %param.39) | copy-start | bytes 2752516
  32.5 16.0 %copy-start.12 = (bf16[1,448,1024]{2,1,0:T(8,128)(2,1)S(1)}, bf16[1,448,1024]{2,1,0:T(8,128)(2,1)}, u32[]{:S(2)}) copy-start(bf16[1,448,1024]{2,1,0:T(8,128)(2,1)} %param.41) | copy-start | bytes 2752516
  69.4 12.4 %all-to-all-start.2 = ((bf16[8,16,256]{2,1,0:T(8,128)(2,1)}), bf16[8,16,256]{2,1,0:T(8,128)(2,1)S(1)}, u32[]{:S(2)}, u32[]{:S(2)}) async-start(bf16[8,16,256]{2,1,0:T(8,128)(2,1)} %reduce-scatter.2.cloned.1.call-done), calls=%async_computation.3 | async-start | bytes 131072 | tf_op jit(solution)/shard_map/all_to_all | solution.py:53
  75.0 0.7 copy-start.10
Sparse Core Ops, SparseCore 0:
  51.2 18.0 reduce-scatter.1
